TPU v7x, 512 devices: a whole 4x8x8 slice. The times are simulated.
512 devices in a mesh: sp: 32 (over z, x), tp: 16 (over y, core).
Axes of the slice: x: 4, y: 8, z: 8, core: 2. Of those that a mesh axis runs over, the one named last changes fastest.
Arguments:
- stream_in: bfloat16 [8192, 2048], P(('sp', 'tp')), may hold values from -6 to 6
- queries: bfloat16 [8192, 4096], P('sp', 'tp'), may hold values from -6 to 6
- key_rows: bfloat16 [8192, 4096], P('sp', 'tp'), may hold values from -6 to 6
- values: bfloat16 [8192, 8192], P('sp', 'tp'), may hold values from -6 to 6
- decay_low: bfloat16 [8192, 16], P('sp'), may hold values from -4 to 4
- decay_matrix: bfloat16 [16, 4096], P(None, 'tp'), may hold values from -1.5 to 1.5
- decay_bias: float32 [4096], P('tp')
- decay_shift: float32 [8192, 16], P('sp', 'tp'), may hold values from -1 to 0
- head_gain: float32 [512], replicated, may hold values from 0.1 to 1.9
- output_matrix: bfloat16 [8192, 2048], P('tp'), may hold values from -0.0625 to 0.0625
- feed_gain: float32 [2048], replicated, may hold values from 0.1 to 1.9
- routes: int32 [8192, 2], P('sp'), may hold values from 0 to 31, all different within a row; in each aligned block of 256 rows (0 to 255, 256 to 511, ...) at most 16 rows name the same one
- route_weights: float32 [8192, 2], P('sp'), may hold values from 0.2 to 1
- expert_gate: bfloat16 [32, 2048, 2816], P('sp', None, 'tp'), may hold values from -0.125 to 0.125
- specialist_widen: bfloat16 [32, 2048, 2816], P('sp', None, 'tp'), may hold values from -0.125 to 0.125
- expert_down: bfloat16 [32, 2816, 2048], P('sp', 'tp'), may hold values from -0.109375 to 0.109375
Outputs:
- layer_out: bfloat16 [8192, 2048], P(('sp', 'tp'))
Inputs may be any that keep to these rules, and one draw needn't show every extreme that they name: `routes`: each row names 2 different experts; within each aligned block of 256 rows no expert is named by more than 16 rows, and in every draw some expert is named by exactly 16 rows of some block.
All inputs are finite; a program needn't handle non-finite values.
Results may differ from a plain program's by a relative error of at most 0.02.
Values may be sent and summed in bfloat16 or wider, within the bound.
A program may use at most 64 MiB of HBM per device.

v0:
```python
import jax
import jax.numpy as jnp
from jax import lax
from jax.sharding import Mesh
from jax.sharding import PartitionSpec as P

HK = 256
HV = 512
TOP = 2
BLK = 128
SP = ("sp_0", "sp_1")
TP = ("tp_0", "tp_1")
SP_TP = ("sp_0", "sp_1", "tp_0", "tp_1")
TEMPER = 16.0
EPSILON = 1e-06
HIGHEST = lax.Precision.HIGHEST


def filled_with(shard, identity):
    return jax.tree.map(
        lambda part, zero: jnp.zeros_like(part) + jnp.asarray(zero, part.dtype), shard, identity
    )


def carried_in(shard, axes, combine, identity):
    before = start = filled_with(shard, identity)
    so_far = shard
    for axis in reversed(axes):
        peers, here = (lax.axis_size(axis), lax.axis_index(axis))
        pieces = jax.tree.map(
            lambda part, kind: lax.all_gather(part.astype(kind), axis),
            so_far,
            (jnp.bfloat16, jnp.bfloat16),
        )
        inside, so_far = (start, start)
        for k in range(peers):
            passed = k < here
            so_far = combine(
                so_far, jax.tree.map(lambda part, own: part[k].astype(own.dtype), pieces, shard)
            )
            inside = jax.tree.map(lambda new, old: jnp.where(passed, new, old), so_far, inside)
        before = combine(inside, before)
    return before


def cut_along(shard, dim, peers):
    before, after = (shard.shape[:dim], shard.shape[dim + 1 :])
    return jnp.moveaxis(shard.reshape(*before, peers, -1, *after), dim, 0)


def sent_and_summed(shard, axis, dim):
    tiles = cut_along(shard, dim, lax.axis_size(axis))
    arrived = lax.all_to_all(tiles, axis, split_axis=0, concat_axis=0, tiled=True)
    return arrived.astype(jnp.float32).sum(axis=0)


def gathered_by_axis(shard, axes, dim):
    for axis in reversed(axes):
        shard = lax.all_gather(shard, axis, axis=dim, tiled=True)
    return shard


def decay_logs(decay_low, decay_matrix, decay_bias, decay_shift, heads):
    before_gate = jnp.dot(decay_low, decay_matrix, preferred_element_type=jnp.float32) + decay_bias
    logged = jax.nn.log_sigmoid(before_gate) / TEMPER
    return logged.reshape(before_gate.shape[0], heads, HK) + decay_shift[:, :, None]


def into_blocks(array):
    length, heads, width = array.shape
    return array.reshape(length // BLK, BLK, heads, width).transpose(2, 0, 1, 3)


def segment_summands(queries, key_rows, values, log_decay):
    inside = jnp.cumsum(log_decay, axis=2)
    final_position = inside[:, :, -1:, :]
    scaled_query = queries * jnp.exp(inside) * HK ** (-0.5)
    scaled_key = key_rows * jnp.exp(-inside)
    end_keys = key_rows * jnp.exp(final_position - inside)
    scores = jnp.einsum("hnid,hnjd->hnij", scaled_query, scaled_key, precision=HIGHEST)
    causal = jnp.tril(jnp.ones((BLK, BLK), jnp.bool_))
    scores = jnp.where(causal, scores, 0.0)
    local_out = jnp.einsum("hnij,hnjv->hniv", scores, values, precision=HIGHEST)
    partial_update = jnp.einsum("hnjd,hnjv->hndv", end_keys, values, precision=HIGHEST)
    return (scaled_query, local_out, partial_update, jnp.exp(final_position[:, :, 0, :]))


def run_blocks(scaled_query, partial_update, block_decay, start):

    def advance(state, pieces):
        query_block, added, decay = pieces
        output = jnp.einsum("hid,hdv->hiv", query_block, state, precision=HIGHEST)
        return (state * decay[:, :, None] + added, output)

    final, outputs = lax.scan(
        advance,
        start,
        (
            jnp.moveaxis(scaled_query, 1, 0),
            jnp.moveaxis(partial_update, 1, 0),
            jnp.moveaxis(block_decay, 1, 0),
        ),
    )
    return (final, jnp.moveaxis(outputs, 0, 1))


def link_states(earlier, later):
    return (earlier[0] * later[0], earlier[1] * later[0][..., None] + later[1])


def pass_state(device_decay, local_state):
    identity = (jnp.ones_like(device_decay), jnp.zeros_like(local_state))
    _, carried = carried_in((device_decay, local_state), SP, link_states, identity)
    return carried


def head_norm(heads_out, head_gain):
    heads = heads_out.shape[0]
    flat = heads_out.transpose(1, 2, 0, 3).reshape(-1, heads, HV)
    normed = flat * lax.rsqrt(jnp.mean(flat * flat, axis=-1, keepdims=True) + EPSILON) * head_gain
    return normed.reshape(-1, heads * HV).astype(jnp.bfloat16)


def root_scale(midstream, gain):
    return (
        midstream
        * lax.rsqrt(jnp.mean(midstream * midstream, axis=-1, keepdims=True) + EPSILON)
        * gain
    ).astype(jnp.bfloat16)


def body(
    stream_in,
    queries,
    key_rows,
    values,
    decay_low,
    decay_matrix,
    decay_bias,
    decay_shift,
    head_gain,
    output_matrix,
    feed_gain,
    routes,
    route_weights,
    expert_gate,
    specialist_widen,
    expert_down,
):
    length = queries.shape[0]
    heads = queries.shape[1] // HK
    sequence_devices = lax.axis_size(SP)
    head_devices = lax.axis_size(TP)
    width = stream_in.shape[1]
    log_decay = decay_logs(decay_low, decay_matrix, decay_bias, decay_shift, heads)

    def shaped(array, channels):
        return into_blocks(array.astype(jnp.float32).reshape(length, heads, channels))

    scaled_query, local_out, partial_update, block_decay = segment_summands(
        shaped(queries, HK), shaped(key_rows, HK), shaped(values, HV), into_blocks(log_decay)
    )
    start = jnp.zeros((heads, HK, HV), jnp.float32)
    device_decay = jnp.prod(block_decay, axis=1)
    local_state, carried_out = run_blocks(scaled_query, partial_update, block_decay, start)
    carried = pass_state(device_decay, local_state)
    shifted = jnp.concatenate([jnp.ones_like(block_decay[:, :1]), block_decay[:, :-1]], axis=1)
    before = jnp.cumprod(shifted, axis=1)
    readout = jnp.einsum(
        "hnid,hdv->hniv", scaled_query * before[:, :, None, :], carried, precision=HIGHEST
    )
    total_out = local_out + carried_out + readout
    mixed = head_norm(total_out, head_gain)
    rows_here = length // head_devices
    attended = sent_and_summed(
        jnp.dot(mixed, output_matrix, preferred_element_type=jnp.float32).astype(jnp.bfloat16),
        TP,
        0,
    )
    midstream = stream_in.astype(jnp.float32) + attended
    normed = root_scale(midstream, feed_gain)
    group = lax.all_gather(normed, TP, axis=0, tiled=True)
    experts = sequence_devices * expert_gate.shape[0]
    capacity = head_devices * max(1, TOP * length // (sequence_devices * head_devices))
    block_slots = capacity // head_devices
    own_index = lax.axis_index(TP)
    flat_routes = routes.reshape(-1)
    expert_index = jnp.arange(experts, dtype=jnp.int32)
    matches = (flat_routes[:, None] == expert_index[None, :]).astype(jnp.int32)
    ranking = jnp.sum((jnp.cumsum(matches, axis=0) - matches) * matches, axis=1)
    slot_member = (ranking[:, None] - 0 == jnp.arange(capacity, dtype=jnp.int32)[None, :]).astype(
        jnp.float32
    )
    table = slot_member[:, :, None] * matches[:, None, :].astype(jnp.float32)
    full_table = table.reshape(length, TOP, capacity * experts)
    selector = jnp.sum(full_table, axis=1).T.astype(jnp.bfloat16)
    filled = jnp.dot(selector, group, preferred_element_type=jnp.float32)
    arrived = lax.all_to_all(
        filled.astype(jnp.bfloat16).reshape(capacity, experts, width),
        SP,
        split_axis=1,
        concat_axis=1,
        tiled=True,
    )
    rows_in = arrived.reshape(-1, width)
    gated = jnp.dot(rows_in, expert_gate[0], preferred_element_type=jnp.float32)
    lifted = jnp.dot(rows_in, specialist_widen[0], preferred_element_type=jnp.float32)
    hidden = (jax.nn.silu(gated) * lifted).astype(jnp.bfloat16)
    summed = sent_and_summed(
        jnp.dot(hidden, expert_down[0], preferred_element_type=jnp.float32).astype(jnp.bfloat16),
        TP,
        0,
    )
    expert_token_rows = summed.astype(jnp.bfloat16).reshape(block_slots, sequence_devices, width)
    returned = lax.all_to_all(expert_token_rows, SP, split_axis=1, concat_axis=1, tiled=True)
    weight_table = jnp.sum(full_table * route_weights.reshape(length, TOP, 1), axis=1)
    own_weights = lax.dynamic_slice_in_dim(weight_table, own_index * rows_here, rows_here, 0)
    piece = gathered_by_axis(returned, TP, 0)
    count = piece.shape[0]
    flat_piece = piece.reshape(count * experts, width).astype(jnp.float32)
    routed = jnp.dot(own_weights, flat_piece, precision=HIGHEST, preferred_element_type=jnp.float32)
    return (midstream + routed).astype(jnp.bfloat16)


def solution(mesh):
    finer = Mesh(mesh.devices.reshape(8, 4, 8, 2), ("sp_0", "sp_1", "tp_0", "tp_1"))
    in_specs = (
        P(SP_TP, None),
        P(SP, TP),
        P(SP, TP),
        P(SP, TP),
        P(SP, None),
        P(None, TP),
        P(TP),
        P(SP, TP),
        P(),
        P(TP, None),
        P(),
        P(SP, None),
        P(SP, None),
        P(SP, None, TP),
        P(SP, None, TP),
        P(SP, TP, None),
    )
    out_specs = P(SP_TP, None)
    return jax.shard_map(body, mesh=finer, in_specs=in_specs, out_specs=out_specs, check_vma=False)
```

profile of v0, /device:TPU:2, one launch (start us, length us, event | category | flops | bytes accessed | tf_op | source)
XLA Modules:
  0.0 369.7 jit_solution(5884363078821731961)
XLA Ops:
  6.5 1.3 fusion.71
  7.8 0.3 reduce_window_sum.28
  8.1 0.9 convert_element_type.550
  9.1 2.6 convolution_bitcast_fusion.1
  11.7 4.6 %while.13 = (s32[]{:T(128)}, f32[1,256,512]{2,1,0:T(8,128)S(1)}, f32[2,1,128,512]{3,2,1,0:T(8,128)}, f32[2,1,256]{2,1,0:T(1,128)S(1)}, f32[2,1,256,512]{3,2,1,0:...) while((s32[]{:T(128)}, f32[1,256,512]{2,1,0:T(8,128)S(1)}, ...), condition=%wide.region_2.3_spmd.clone, body=%wide.region_1.2_spmd.clone.sunk | while | flops 201850880 | bytes 2494568 | solution.py:95
  11.7 1.2 fusion.144
  12.8 1.2 bitcast_add_fusion.2
  14.0 1.1 fusion.144
  15.2 1.2 bitcast_add_fusion.2
  16.3 0.7 convert_element_type.561
  17.1 0.0 all-gather.14.cloned.1.call-update
  17.1 0.0 all-gather.8.cloned.1.call-start
  17.2 12.9 %all-gather.2 = bf16[4,1,256]{2,1,0:T(2,128)(2,1)S(1)} all-gather(bf16[1,1,256]{2,1,0:T(2,128)(2,1)S(1)} %reshape.1207), channel_id=2, replica_groups=mesh['sp_0'=8,'sp_1'=4,'tp_0'=8,'tp_1'=2] {'sp_1'}, dimensions={0}, use_global_device_ids=true | all-gather | bytes 2560 | tf_op jit(solution)/shard_map/all_gather | solution.py:31
  30.0 20.1 %all-gather.14.cloned.1.call-done = bf16[4,256,512]{2,1,0:T(8,128)(2,1)} async-done(((bf16[1,256,512]{2,1,0:T(8,128)(2,1)}), bf16[4,256,512]{2,1,0:T(8,128)(2,1)}) %all-gather.14.cloned.1.call-update) | async-done | bytes 1048592 | tf_op jit(solution)/shard_map/all_gather | solution.py:31
  50.2 2.2 fusion.25
  52.3 0.0 all-gather.8.cloned.1.call-update
  52.3 0.0 all-gather.10.cloned.1.call-start
  52.6 17.3 %all_gather.28 = bf16[8,1,256]{2,1,0:T(2,128)(2,1)S(1)} all-gather(bf16[1,1,256]{2,1,0:T(2,128)(2,1)S(1)} %reshape.1214), channel_id=1, replica_groups=mesh['sp_0'=8,'sp_1'=4,'tp_0'=8,'tp_1'=2] {'sp_0'}, dimensions={0}, use_global_device_ids=true | all-gather | bytes 4608 | tf_op jit(solution)/shard_map/all_gather | solution.py:31
  69.9 0.5 convolution_select_fusion
  70.3 27.7 %all-gather.8.cloned.1.call-done = bf16[8,1,256,512]{3,2,1,0:T(8,128)(2,1)} async-done(((bf16[1,1,256,512]{3,2,1,0:T(8,128)(2,1)}), bf16[8,1,256,512]{3,2,1,0:T(8,128)(2,1)}) %all-gather.8.cloned.1.call-update) | async-done | bytes 2097168 | tf_op jit(solution)/shard_map/all_gather | solution.py:31
  98.0 3.5 fusion.35
  101.6 0.5 multiply_reduce_fusion.1
  102.1 0.1 fusion.53
  102.2 0.7 convolution_convert_fusion.2
  102.9 0.0 copy-start.3
  103.0 33.9 %all_to_all.20 = bf16[16,16,2048]{2,1,0:T(8,128)(2,1)S(1)} all-to-all(bf16[16,16,2048]{2,1,0:T(8,128)(2,1)S(1)} %bitcast.272), channel_id=1, replica_groups=mesh['sp_0'=8,'sp_1'=4,'tp_0'=8,'tp_1'=2] {'tp_0','tp_1'}, dimensions={0} | all-to-all | bytes 2097152 | tf_op jit(solution)/shard_map/all_to_all | solution.py:53
  136.9 0.1 convert_reduce_fusion
  137.1 0.1 multiply_reduce_fusion.2
  137.2 0.7 multiply_convert_fusion
  137.9 0.0 all-gather.10.cloned.1.call-update
  138.0 0.2 all-gather.12.cloned.1.call-start
  138.2 0.1 copy.42
  138.4 0.1 eq.50
  138.5 0.1 eq.46
  138.7 1.2 reduce-window.9
  139.8 0.2 slice_reduce_fusion
  140.1 0.1 copy.45
  140.2 0.1 fusion.117
  140.3 0.1 fusion.96
  140.5 4.1 %broadcast_multiply_fusion = f32[512,16,32]{2,1,0:T(8,128)} fusion(f32[512,32]{1,0:T(8,128)S(1)} %copy.45, f32[512,16]{1,0:T(8,128)S(1)} %fusion.96), kind=kLoop, calls=%fused_computation.17 | loop fusion | flops 262144 | bytes 1146880 | tf_op jit(solution)/shard_map/mul | solution.py:194
  144.6 3.9 %mul.567 = f32[256,2,512]{2,1,0:T(2,128)S(1)} reshape(f32[512,16,32]{2,1,0:T(8,128)} %broadcast_multiply_fusion) | data formatting | bytes 2097152 | tf_op jit(solution)/shard_map/mul | solution.py:194
  148.4 0.8 copy.46
  149.2 4.2 %multiply_reduce_fusion = (f32[256,512]{1,0:T(8,128)}, bf16[256,512]{1,0:T(8,128)(2,1)S(1)}) fusion(f32[256,2,512]{2,1,0:T(2,128)S(1)} %mul.567, f32[256,2]{1,0:T(8,128)} %copy.46), kind=kLoop, calls=%fused_computation.27 | loop fusion | flops 524288 | bytes 1837056 | tf_op jit(solution)/shard_map/reduce_sum | solution.py:216
  153.4 21.1 %all-gather.10.cloned.1.call-done = bf16[256,2048]{1,0:T(8,128)(2,1)} async-done(((bf16[16,2048]{1,0:T(8,128)(2,1)}), bf16[256,2048]{1,0:T(8,128)(2,1)}) %all-gather.10.cloned.1.call-update) | async-done | bytes 1048592 | tf_op jit(solution)/shard_map/all_gather | solution.py:182
  174.5 2.0 convolution_convert_fusion.1
  176.5 1.2 copy.47
  177.6 61.2 %all_to_all.21 = bf16[16,32,2048]{2,0,1:T(8,128)(2,1)S(1)} all-to-all(bf16[16,32,2048]{2,0,1:T(8,128)(2,1)S(1)} %copy.47), channel_id=1, replica_groups=mesh['sp_0'=8,'sp_1'=4,'tp_0'=8,'tp_1'=2] {'sp_0','sp_1'}, dimensions={1} | all-to-all | bytes 4194304 | tf_op jit(solution)/shard_map/all_to_all | solution.py:198
  238.9 1.2 copy.48
  240.0 1.3 copy-done.1
  241.3 1.6 fusion.16
  242.9 4.8 %convolution_convert_fusion = bf16[512,2048]{1,0:T(8,128)(2,1)} fusion(bf16[512,2048]{1,0:T(8,128)(2,1)} %bitcast.277, bf16[1,176,2048]{2,1,0:T(8,128)(2,1)S(1)} %copy-done.13, bf16[1,2048,176]{1,2,0:T(8,128)(2,1)} %param.32, f32[512,176]{0,1:T(8,128)} %fusion.16), kind=kOutput, calls=%fused_computation.12 | convolution fusion | flops 739786752 | bytes 5996544 | tf_op jit(solution)/shard_map/dot_general | solution.py:210
  247.7 54.5 %all_to_all.22 = bf16[16,32,2048]{2,1,0:T(8,128)(2,1)} all-to-all(bf16[16,32,2048]{2,1,0:T(8,128)(2,1)} %bitcast.278), channel_id=1, replica_groups=mesh['sp_0'=8,'sp_1'=4,'tp_0'=8,'tp_1'=2] {'tp_0','tp_1'}, dimensions={0} | all-to-all | bytes 4194304 | tf_op jit(solution)/shard_map/all_to_all | solution.py:53
  302.2 2.0 reduce_sum.72
  304.2 0.2 copy.58
  304.4 0.5 broadcast.665
  304.9 1.4 reduce.8
  306.3 0.1 reshape.1223
  306.4 14.6 %all_to_all.23 = bf16[32,2,1024]{2,1,0:T(2,128)(2,1)S(1)} all-to-all(bf16[32,2,1024]{2,1,0:T(2,128)(2,1)S(1)} %reshape.1223), channel_id=1, replica_groups=mesh['sp_0'=8,'sp_1'=4,'tp_0'=8,'tp_1'=2] {'sp_0','sp_1'}, dimensions={0} | all-to-all | bytes 262144 | tf_op jit(solution)/shard_map/all_to_all | solution.py:215
  320.9 0.1 reshape.1224
  321.0 0.1 copy.50
  321.1 2.2 all_gather.33
  323.3 0.0 all-gather.12.cloned.1.call-update
  323.3 36.7 %all-gather.12.cloned.1.call-done = bf16[16,32,2048]{2,1,0:T(8,128)(2,1)} async-done(((bf16[2,32,2048]{2,1,0:T(8,128)(2,1)}), bf16[16,32,2048]{2,1,0:T(8,128)(2,1)}) %all-gather.12.cloned.1.call-update) | async-done | bytes 2097168 | tf_op jit(solution)/shard_map/all_gather | solution.py:59
  360.0 3.2 fusion.9
  (52 shorter events, 0.4 us)
Async XLA Ops:
  6.5 95.7 %copy-start = (bf16[512,2048]{1,0:T(8,128)(2,1)S(1)}, bf16[512,2048]{1,0:T(8,128)(2,1)}, u32[]{:S(2)}) copy-start(bf16[512,2048]{1,0:T(8,128)(2,1)} %param.27) | copy-start | bytes 6291460
  6.5 2.5 copy-start.7
  6.5 43.6 %all-gather.14.cloned.1.call-start = ((), (), s32[]{:S(2)}) async-start(), calls=%async_computation.7 | async-start | bytes 1310720 | tf_op jit(solution)/shard_map/all_gather | solution.py:31
  16.3 36.2 %copy-start.6 = (bf16[256,256]{1,0:T(8,128)(2,1)S(1)}, bf16[256,256]{1,0:T(8,128)(2,1)}, u32[]{:S(2)}) copy-start(bf16[256,256]{1,0:T(8,128)(2,1)} %param.19) | copy-start | bytes 393220
  17.1 80.9 %all-gather.8.cloned.1.call-start = ((), (), s32[]{:S(2)}) async-start(), calls=%async_computation.4 | async-start | bytes 2359296 | tf_op jit(solution)/shard_map/all_gather | solution.py:31
  52.3 122.2 %all-gather.10.cloned.1.call-start = ((), (), s32[]{:S(2)}) async-start(), calls=%async_computation.5 | async-start | bytes 1114112 | tf_op jit(solution)/shard_map/all_gather | solution.py:182
  98.0 3.5 copy-start.2
  98.0 3.5 copy-start.5
  98.0 4.0 %copy-start.9 = (f32[512]{0:T(512)S(1)}, f32[512]{0:T(512)}, u32[]{:S(2)}) copy-start(f32[512]{0:T(512)} %param.26) | copy-start | bytes 6148
  102.9 34.1 %copy-start.3 = (bf16[16,2048]{1,0:T(8,128)(2,1)S(1)}, bf16[16,2048]{1,0:T(8,128)(2,1)}, u32[]{:S(2)}) copy-start(bf16[16,2048]{1,0:T(8,128)(2,1)} %param.18) | copy-start | bytes 196612
  102.9 34.3 %copy-start.8 = (f32[2048]{0:T(1024)S(1)}, f32[2048]{0:T(1024)}, u32[]{:S(2)}) copy-start(f32[2048]{0:T(1024)} %param.28) | copy-start | bytes 24580
  103.0 35.2 %copy-start.10 = (s32[256,2]{0,1:T(2,128)S(1)}, s32[256,2]{0,1:T(2,128)}, u32[]{:S(2)}) copy-start(s32[256,2]{0,1:T(2,128)} %param.29) | copy-start | bytes 6148
  138.0 222.1 %all-gather.12.cloned.1.call-start = ((), (), s32[]{:S(2)}) async-start(), calls=%async_computation.6 | async-start | bytes 2359296 | tf_op jit(solution)/shard_map/all_gather | solution.py:59
  144.6 3.9 %copy-start.11 = (f32[256,2]{0,1:T(2,128)S(1)}, f32[256,2]{0,1:T(2,128)}, u32[]{:S(2)}) copy-start(f32[256,2]{0,1:T(2,128)} %param.30) | copy-start | bytes 6148
  238.9 2.5 copy-start.12
  240.0 1.3 copy-start.1
  241.3 1.6 copy-start.13
  302.2 57.9 %copy-start.4 = (bf16[16,2048]{1,0:T(8,128)(2,1)S(1)}, bf16[16,2048]{1,0:T(8,128)(2,1)}, u32[]{:S(2)}) copy-start(bf16[16,2048]{1,0:T(8,128)(2,1)} %param.18) | copy-start | bytes 196612
Sparse Core Ops, SparseCore 0:
  17.2 32.9 all-gather.13
  52.5 45.5 all-gather.7
  138.1 36.3 all-gather.9
  323.5 36.5 all-gather.11
where the time goes:
time: 370 us
  blocking collectives  197 us (53%)
  waiting for transfers between devices  106 us (29%)
  matrix products  22.8 us (6%)
  other arithmetic  20.8 us (6%)
  between operations  13.5 us (4%)
  local copies, waits for them, and re-layouts  10.1 us (3%)
    all_to_all x2, blocking collectives, sent_and_summed(): lax.all_to_all(tiles, axis, split_axis=0, concat_axis=0, tiled=True)  88.4 us
    all_to_all x1, blocking collectives, body(): lax.all_to_all(filled.astype(jnp.bfloat16).reshape(capacity, experts, wid...  61.2 us
    all_gather x2, waiting for transfers between devices, carried_in(): lax.all_gather(part.astype(kind), axis)  47.8 us
    all_gather x1, waiting for transfers between devices, gathered_by_axis(): shard = lax.all_gather(shard, axis, axis=dim, tiled=True)  36.7 us
    all_gather x2, blocking collectives, carried_in(): lax.all_gather(part.astype(kind), axis)  30.1 us
    all_gather x1, waiting for transfers between devices, body(): group = lax.all_gather(normed, TP, axis=0, tiled=True)  21.1 us
    all_to_all x1, blocking collectives, body(): lax.all_to_all(expert_token_rows, SP, split_axis=1, concat_axis=1, tiled=...  14.6 us
  transfers between devices with their start and end apart: 4, of which 4 were waited for; matrix products, arithmetic and copies ran while one was open for 4% of the time, Pallas kernels for 0%

commit v1 on v0

--- a/solution.py
+++ b/solution.py
@@ -179,7 +179,9 @@
     )
     midstream = stream_in.astype(jnp.float32) + attended
     normed = root_scale(midstream, feed_gain)
-    group = lax.all_gather(normed, TP, axis=0, tiled=True)
+    group = jnp.concatenate(
+        lax.all_to_all(jnp.stack([normed] * lax.axis_size(TP)), TP, 0, 0), axis=0
+    )
     experts = sequence_devices * expert_gate.shape[0]
     capacity = head_devices * max(1, TOP * length // (sequence_devices * head_devices))
     block_slots = capacity // head_devices

time: 370 us -> 362 us (0.978)
  waiting for transfers between devices: 106 us -> 95.7 us
  starting transfers between devices: 0.31 us -> 4.62 us
    all_gather x1 -> x0, waiting for transfers between devices: 21.1 us -> none  [body(): group = lax.all_gather(normed, TP, axis=0, tiled=True)]
    all_to_all x0 -> x1, waiting for transfers between devices: none -> 11 us  [body(): lax.all_to_all(jnp.stack([normed] * lax.axis_size(TP)), TP, 0, 0)]
    all_to_all x0 -> x1, starting transfers between devices: none -> 4.35 us  [body(): lax.all_to_all(jnp.stack([normed] * lax.axis_size(TP)), TP, 0, 0)]
where the time goes in v1:
time: 362 us
  blocking collectives  194 us (54%)
  waiting for transfers between devices  95.7 us (26%)
  matrix products  22.8 us (6%)
  other arithmetic  20.2 us (6%)
  between operations  13.5 us (4%)
  local copies, waits for them, and re-layouts  11.2 us (3%)
  starting transfers between devices  4.62 us (1%)
    all_to_all x2, blocking collectives, sent_and_summed(): lax.all_to_all(tiles, axis, split_axis=0, concat_axis=0, tiled=True)  88.5 us
    all_to_all x1, blocking collectives, body(): lax.all_to_all(filled.astype(jnp.bfloat16).reshape(capacity, experts, wid...  58.3 us
    all_gather x2, waiting for transfers between devices, carried_in(): lax.all_gather(part.astype(kind), axis)  47.9 us
    all_gather x1, waiting for transfers between devices, gathered_by_axis(): shard = lax.all_gather(shard, axis, axis=dim, tiled=True)  36.7 us
    all_gather x2, blocking collectives, carried_in(): lax.all_gather(part.astype(kind), axis)  30.1 us
    all_to_all x1, blocking collectives, body(): lax.all_to_all(expert_token_rows, SP, split_axis=1, concat_axis=1, tiled=...  14.6 us
    all_to_all x1, waiting for transfers between devices, body(): lax.all_to_all(jnp.stack([normed] * lax.axis_size(TP)), TP, 0, 0)  11 us
  transfers between devices with their start and end apart: 4, of which 4 were waited for; matrix products, arithmetic and copies ran while one was open for 4% of the time, Pallas kernels for 0%

profile of v1, /device:TPU:2, one launch (start us, length us, event | category | flops | bytes accessed | tf_op | source)
XLA Modules:
  0.0 361.7 jit_solution(1803744849385457798)
XLA Ops:
  6.5 1.3 fusion.71
  7.8 0.3 reduce_window_sum.28
  8.1 0.9 convert_element_type.550
  9.1 2.6 convolution_bitcast_fusion.1
  11.7 4.6 %while.13 = (s32[]{:T(128)}, f32[1,256,512]{2,1,0:T(8,128)S(1)}, f32[2,1,128,512]{3,2,1,0:T(8,128)}, f32[2,1,256]{2,1,0:T(1,128)S(1)}, f32[2,1,256,512]{3,2,1,0:...) while((s32[]{:T(128)}, f32[1,256,512]{2,1,0:T(8,128)S(1)}, ...), condition=%wide.region_2.3_spmd.clone, body=%wide.region_1.2_spmd.clone.sunk | while | flops 201850880 | bytes 2494568 | solution.py:95
  11.7 1.2 fusion.144
  12.8 1.2 bitcast_add_fusion.2
  14.0 1.1 fusion.144
  15.2 1.2 bitcast_add_fusion.2
  16.3 0.7 convert_element_type.561
  17.1 0.0 all-gather.11.cloned.1.call-update
  17.1 0.0 all-gather.7.cloned.1.call-start
  17.2 12.9 %all-gather.2 = bf16[4,1,256]{2,1,0:T(2,128)(2,1)S(1)} all-gather(bf16[1,1,256]{2,1,0:T(2,128)(2,1)S(1)} %reshape.1213), channel_id=2, replica_groups=mesh['sp_0'=8,'sp_1'=4,'tp_0'=8,'tp_1'=2] {'sp_1'}, dimensions={0}, use_global_device_ids=true | all-gather | bytes 2560 | tf_op jit(solution)/shard_map/all_gather | solution.py:31
  30.0 20.1 %all-gather.11.cloned.1.call-done = bf16[4,256,512]{2,1,0:T(8,128)(2,1)} async-done(((bf16[1,256,512]{2,1,0:T(8,128)(2,1)}), bf16[4,256,512]{2,1,0:T(8,128)(2,1)}) %all-gather.11.cloned.1.call-update) | async-done | bytes 1048592 | tf_op jit(solution)/shard_map/all_gather | solution.py:31
  50.2 2.2 fusion.25
  52.3 0.0 all-gather.7.cloned.1.call-update
  52.5 17.3 %all_gather.25 = bf16[8,1,256]{2,1,0:T(2,128)(2,1)S(1)} all-gather(bf16[1,1,256]{2,1,0:T(2,128)(2,1)S(1)} %reshape.1220), channel_id=1, replica_groups=mesh['sp_0'=8,'sp_1'=4,'tp_0'=8,'tp_1'=2] {'sp_0'}, dimensions={0}, use_global_device_ids=true | all-gather | bytes 4608 | tf_op jit(solution)/shard_map/all_gather | solution.py:31
  69.8 0.5 convolution_select_fusion
  70.3 27.8 %all-gather.7.cloned.1.call-done = bf16[8,1,256,512]{3,2,1,0:T(8,128)(2,1)} async-done(((bf16[1,1,256,512]{3,2,1,0:T(8,128)(2,1)}), bf16[8,1,256,512]{3,2,1,0:T(8,128)(2,1)}) %all-gather.7.cloned.1.call-update) | async-done | bytes 2097168 | tf_op jit(solution)/shard_map/all_gather | solution.py:31
  98.1 3.5 fusion.35
  101.6 0.5 multiply_reduce_fusion.1
  102.2 0.1 fusion.53
  102.3 0.7 convolution_convert_fusion.2
  103.0 0.0 copy-start.3
  103.0 34.0 %all_to_all.25 = bf16[16,16,2048]{2,1,0:T(8,128)(2,1)S(1)} all-to-all(bf16[16,16,2048]{2,1,0:T(8,128)(2,1)S(1)} %bitcast.273), channel_id=1, replica_groups=mesh['sp_0'=8,'sp_1'=4,'tp_0'=8,'tp_1'=2] {'tp_0','tp_1'}, dimensions={0} | all-to-all | bytes 2097152 | tf_op jit(solution)/shard_map/all_to_all | solution.py:53
  137.0 0.1 convert_reduce_fusion
  137.2 0.1 multiply_reduce_fusion.2
  137.3 0.1 multiply_convert_fusion
  137.4 1.1 stack.2
  138.6 4.4 %all-to-all-start.1 = ((bf16[16,16,2048]{2,1,0:T(8,128)(2,1)}), bf16[16,16,2048]{2,1,0:T(8,128)(2,1)}, u32[]{:S(2)}, u32[]{:S(2)}) async-start(bf16[16,16,2048]{2,1,0:T(8,128)(2,1)} %stack.2), calls=%async_computation.1 | async-start | bytes 2097152 | tf_op jit(solution)/shard_map/all_to_all | solution.py:183
  142.9 0.2 all-gather.9.cloned.1.call-start
  143.2 0.1 copy.42
  143.3 0.1 eq.50
  143.4 0.1 eq.46
  143.6 1.2 reduce-window.9
  144.8 0.2 slice_reduce_fusion
  145.1 0.1 copy.45
  145.2 0.1 fusion.117
  145.3 0.1 fusion.96
  145.4 4.1 %broadcast_multiply_fusion = f32[512,16,32]{2,1,0:T(8,128)} fusion(f32[512,32]{1,0:T(8,128)S(1)} %copy.45, f32[512,16]{1,0:T(8,128)S(1)} %fusion.96), kind=kLoop, calls=%fused_computation.17 | loop fusion | flops 262144 | bytes 1146880 | tf_op jit(solution)/shard_map/mul | solution.py:196
  149.5 3.9 %mul.567 = f32[256,2,512]{2,1,0:T(2,128)S(1)} reshape(f32[512,16,32]{2,1,0:T(8,128)} %broadcast_multiply_fusion) | data formatting | bytes 2097152 | tf_op jit(solution)/shard_map/mul | solution.py:196
  153.4 0.8 copy.46
  154.2 4.2 %multiply_reduce_fusion = (f32[256,512]{1,0:T(8,128)}, bf16[256,512]{1,0:T(8,128)(2,1)S(1)}) fusion(f32[256,2,512]{2,1,0:T(2,128)S(1)} %mul.567, f32[256,2]{1,0:T(8,128)} %copy.46), kind=kLoop, calls=%fused_computation.27 | loop fusion | flops 524288 | bytes 1837056 | tf_op jit(solution)/shard_map/reduce_sum | solution.py:218
  158.3 11.0 %all-to-all-done.1 = bf16[16,16,2048]{2,1,0:T(8,128)(2,1)} async-done(((bf16[16,16,2048]{2,1,0:T(8,128)(2,1)}), bf16[16,16,2048]{2,1,0:T(8,128)(2,1)}, u32[]{:S(2)}, u32[]{:S(2)}) %all-to-all-start.1) | async-done | bytes 1048608 | tf_op jit(solution)/shard_map/all_to_all | solution.py:183
  169.3 2.0 convolution_convert_fusion.1
  171.3 1.2 copy.47
  172.5 58.3 %all_to_all.26 = bf16[16,32,2048]{2,0,1:T(8,128)(2,1)S(1)} all-to-all(bf16[16,32,2048]{2,0,1:T(8,128)(2,1)S(1)} %copy.47), channel_id=1, replica_groups=mesh['sp_0'=8,'sp_1'=4,'tp_0'=8,'tp_1'=2] {'sp_0','sp_1'}, dimensions={1} | all-to-all | bytes 4194304 | tf_op jit(solution)/shard_map/all_to_all | solution.py:200
  230.7 1.2 copy.48
  231.9 1.3 copy-done.1
  233.2 1.6 fusion.16
  234.8 4.8 %convolution_convert_fusion = bf16[512,2048]{1,0:T(8,128)(2,1)} fusion(bf16[512,2048]{1,0:T(8,128)(2,1)} %bitcast.278, bf16[1,176,2048]{2,1,0:T(8,128)(2,1)S(1)} %copy-done.13, bf16[1,2048,176]{1,2,0:T(8,128)(2,1)} %param.32, f32[512,176]{0,1:T(8,128)} %fusion.16), kind=kOutput, calls=%fused_computation.12 | convolution fusion | flops 739786752 | bytes 5996544 | tf_op jit(solution)/shard_map/dot_general | solution.py:212
  239.5 54.5 %all_to_all.27 = bf16[16,32,2048]{2,1,0:T(8,128)(2,1)} all-to-all(bf16[16,32,2048]{2,1,0:T(8,128)(2,1)} %bitcast.279), channel_id=1, replica_groups=mesh['sp_0'=8,'sp_1'=4,'tp_0'=8,'tp_1'=2] {'tp_0','tp_1'}, dimensions={0} | all-to-all | bytes 4194304 | tf_op jit(solution)/shard_map/all_to_all | solution.py:53
  294.1 2.0 reduce_sum.72
  296.1 0.2 copy.58
  296.3 0.5 broadcast.667
  296.8 1.4 reduce.8
  298.2 0.1 reshape.1229
  298.3 14.6 %all_to_all.28 = bf16[32,2,1024]{2,1,0:T(2,128)(2,1)S(1)} all-to-all(bf16[32,2,1024]{2,1,0:T(2,128)(2,1)S(1)} %reshape.1229), channel_id=1, replica_groups=mesh['sp_0'=8,'sp_1'=4,'tp_0'=8,'tp_1'=2] {'sp_0','sp_1'}, dimensions={0} | all-to-all | bytes 262144 | tf_op jit(solution)/shard_map/all_to_all | solution.py:217
  312.9 0.1 reshape.1230
  313.0 0.1 copy.50
  313.1 2.2 all_gather.29
  315.2 0.0 all-gather.9.cloned.1.call-update
  315.3 36.7 %all-gather.9.cloned.1.call-done = bf16[16,32,2048]{2,1,0:T(8,128)(2,1)} async-done(((bf16[2,32,2048]{2,1,0:T(8,128)(2,1)}), bf16[16,32,2048]{2,1,0:T(8,128)(2,1)}) %all-gather.9.cloned.1.call-update) | async-done | bytes 2097168 | tf_op jit(solution)/shard_map/all_gather | solution.py:59
  352.0 3.2 fusion.9
  (52 shorter events, 0.4 us)
Async XLA Ops:
  6.5 95.7 %copy-start = (bf16[512,2048]{1,0:T(8,128)(2,1)S(1)}, bf16[512,2048]{1,0:T(8,128)(2,1)}, u32[]{:S(2)}) copy-start(bf16[512,2048]{1,0:T(8,128)(2,1)} %param.27) | copy-start | bytes 6291460
  6.5 2.5 copy-start.7
  6.5 43.6 %all-gather.11.cloned.1.call-start = ((), (), s32[]{:S(2)}) async-start(), calls=%async_computation.7 | async-start | bytes 1310720 | tf_op jit(solution)/shard_map/all_gather | solution.py:31
  16.3 36.2 %copy-start.6 = (bf16[256,256]{1,0:T(8,128)(2,1)S(1)}, bf16[256,256]{1,0:T(8,128)(2,1)}, u32[]{:S(2)}) copy-start(bf16[256,256]{1,0:T(8,128)(2,1)} %param.19) | copy-start | bytes 393220
  17.1 81.0 %all-gather.7.cloned.1.call-start = ((), (), s32[]{:S(2)}) async-start(), calls=%async_computation.5 | async-start | bytes 2359296 | tf_op jit(solution)/shard_map/all_gather | solution.py:31
  98.1 3.5 copy-start.2
  98.1 3.5 copy-start.5
  98.1 4.0 %copy-start.9 = (f32[512]{0:T(512)S(1)}, f32[512]{0:T(512)}, u32[]{:S(2)}) copy-start(f32[512]{0:T(512)} %param.26) | copy-start | bytes 6148
  103.0 34.1 %copy-start.3 = (bf16[16,2048]{1,0:T(8,128)(2,1)S(1)}, bf16[16,2048]{1,0:T(8,128)(2,1)}, u32[]{:S(2)}) copy-start(bf16[16,2048]{1,0:T(8,128)(2,1)} %param.18) | copy-start | bytes 196612
  103.0 34.3 %copy-start.8 = (f32[2048]{0:T(1024)S(1)}, f32[2048]{0:T(1024)}, u32[]{:S(2)}) copy-start(f32[2048]{0:T(1024)} %param.28) | copy-start | bytes 24580
  137.2 6.0 %copy-start.10 = (s32[256,2]{0,1:T(2,128)S(1)}, s32[256,2]{0,1:T(2,128)}, u32[]{:S(2)}) copy-start(s32[256,2]{0,1:T(2,128)} %param.29) | copy-start | bytes 6148
  138.6 30.8 %all-to-all-start.1 = ((bf16[16,16,2048]{2,1,0:T(8,128)(2,1)}), bf16[16,16,2048]{2,1,0:T(8,128)(2,1)}, u32[]{:S(2)}, u32[]{:S(2)}) async-start(bf16[16,16,2048]{2,1,0:T(8,128)(2,1)} %stack.2), calls=%async_computation.1 | async-start | bytes 2097152 | tf_op jit(solution)/shard_map/all_to_all | solution.py:183
  142.9 209.0 %all-gather.9.cloned.1.call-start = ((), (), s32[]{:S(2)}) async-start(), calls=%async_computation.6 | async-start | bytes 2359296 | tf_op jit(solution)/shard_map/all_gather | solution.py:59
  149.5 3.9 %copy-start.11 = (f32[256,2]{0,1:T(2,128)S(1)}, f32[256,2]{0,1:T(2,128)}, u32[]{:S(2)}) copy-start(f32[256,2]{0,1:T(2,128)} %param.30) | copy-start | bytes 6148
  230.7 2.5 copy-start.12
  231.9 1.3 copy-start.1
  233.2 1.6 copy-start.13
  294.1 57.9 %copy-start.4 = (bf16[16,2048]{1,0:T(8,128)(2,1)S(1)}, bf16[16,2048]{1,0:T(8,128)(2,1)}, u32[]{:S(2)}) copy-start(bf16[16,2048]{1,0:T(8,128)(2,1)} %param.18) | copy-start | bytes 196612
Sparse Core Ops, SparseCore 0:
  17.2 32.9 all-gather.10
  52.5 45.5 all-gather.6
  315.4 36.5 all-gather.8
